TPU v7x, 32 devices: a whole 2x2x4 slice. The times are simulated.
32 devices in a mesh: rep: 2 (over x), fs: 8 (over z, y), tp: 2 (over core).
Axes of the slice: x: 2, y: 2, z: 4, core: 2. Of those that a mesh axis runs over, the one named last changes fastest.
Arguments:
- tokens: bfloat16 [4096, 2048], P(('rep', 'fs')), may hold values from -6 to 6
- ffn_gate: bfloat16 [2048, 5632], P('fs', 'tp'), may hold values from -0.125 to 0.125
- ffn_up: bfloat16 [2048, 5632], P('fs', 'tp'), may hold values from -0.125 to 0.125
- ffn_down: bfloat16 [5632, 2048], P('tp', 'fs'), may hold values from -0.3125 to 0.3125
- query_proj: bfloat16 [2048, 512], P('fs', 'tp'), may hold values from -0.125 to 0.125
- key_proj: bfloat16 [2048, 512], P('fs', 'tp'), may hold values from -0.125 to 0.125
- value_proj: bfloat16 [2048, 1024], P('fs', 'tp'), may hold values from -0.125 to 0.125
- outgate_proj: bfloat16 [2048, 1024], P('fs', 'tp'), may hold values from -0.125 to 0.125
- output_proj: bfloat16 [1024, 2048], P('tp', 'fs'), may hold values from -0.375 to 0.375
- rank_down: bfloat16 [2048, 16], replicated, may hold values from -0.1875 to 0.1875
- rank_up: bfloat16 [16, 512], replicated, may hold values from -3 to 3
- decay_bias: float32 [512], replicated, may hold values from -0.5 to 8
- head_gain: float32 [1024], replicated, may hold values from 0.1 to 1.9
- norm_gain: float32 [3, 2048], replicated, may hold values from 0.1 to 1.9
- norm_bias: float32 [3, 2048], replicated, may hold values from -2 to 2
Outputs:
- layer_out: bfloat16 [4096, 2048], P(('rep', 'fs'))
All inputs are finite; a program needn't handle non-finite values.
Results may differ from a plain program's by a relative error of at most 0.024.
Values may be sent and summed in bfloat16 or wider, within the bound.
No kernel may reach another device: no remote copies, remote signals or barrier semaphores. Data moves between devices by JAX's collectives and lax.ppermute only.
A program may use at most 128 MiB of HBM per device.

v0:
```python
import jax
import jax.numpy as jnp
from jax import lax
from jax.sharding import PartitionSpec as P

DK = 64
DV = 128
BLOCK = 64
EPSILON = 1e-05
HEAD_FLOOR = 1.0
RESIDUAL_SCALE = 2.0**0.5
GATE_SOFTNESS = 16.0
FULL_ACCURACY = lax.Precision.HIGHEST


def layer_norm(summed, norm_gain, norm_shift):
    centred = summed - jnp.mean(summed, -1, keepdims=True)
    spread = jnp.mean(centred * centred, -1, keepdims=True)
    return (centred * lax.rsqrt(spread + EPSILON) * norm_gain + norm_shift).astype(jnp.bfloat16)


def gla_heads(queries, keys_rows, values, decay_logarithm):
    length, head_count, key_width = queries.shape
    value_width = values.shape[-1]
    block_count = length // BLOCK

    def blocks(array):
        return array.reshape(block_count, BLOCK, head_count, array.shape[-1])

    causal = jnp.tril(jnp.ones((BLOCK, BLOCK), bool))[:, :, None, None]

    def advance(running_state, inputs):
        query_block, key_block, value_block, decay_blk = inputs
        decay_prefix = jnp.cumsum(decay_blk, axis=0)
        spread = decay_prefix[:, None] - decay_prefix[None, :]
        weight = jnp.exp(jnp.where(causal, spread, -jnp.inf))
        scores = jnp.einsum(
            "lshk,lhk,shk->hls", weight, query_block, key_block, precision=FULL_ACCURACY
        )
        within = jnp.einsum("hls,shv->lhv", scores, value_block, precision=FULL_ACCURACY)
        carried_over = jnp.einsum(
            "zew,ewa->zea",
            query_block * jnp.exp(decay_prefix),
            running_state,
            precision=FULL_ACCURACY,
        )
        block_finish = decay_prefix[-1]
        running_state = jnp.exp(block_finish)[:, :, None] * running_state + jnp.einsum(
            "oct,ocy->cty",
            key_block * jnp.exp(block_finish[None] - decay_prefix),
            value_block,
            precision=FULL_ACCURACY,
        )
        return (running_state, within + carried_over)

    initial = jnp.zeros((head_count, key_width, value_width), jnp.float32)
    _, outputs = lax.scan(
        advance,
        initial,
        (blocks(queries), blocks(keys_rows), blocks(values), blocks(decay_logarithm)),
    )
    return outputs.reshape(length, head_count, value_width)


def settle(partial_value, residual_rows, factor, norm_gain, norm_shift):
    summed = lax.psum(partial_value.astype(jnp.bfloat16), "tp").astype(jnp.float32)
    return layer_norm(
        RESIDUAL_SCALE * residual_rows.astype(jnp.float32) + factor * summed, norm_gain, norm_shift
    )


def channel_mix(normed, gate_full, up_full, down_full):
    gate_rows = jnp.dot(normed, gate_full, preferred_element_type=jnp.float32)
    up_rows = jnp.dot(normed, up_full, preferred_element_type=jnp.float32)
    hidden = (jax.nn.silu(gate_rows) * up_rows).astype(jnp.bfloat16)
    return jnp.dot(hidden, down_full, preferred_element_type=jnp.float32)


def per_device(
    tokens,
    ffn_gate,
    ffn_up,
    ffn_down,
    query_proj,
    key_proj,
    value_proj,
    outgate_proj,
    output_proj,
    rank_down,
    rank_up,
    decay_bias,
    head_gain,
    norm_gain,
    norm_bias,
):
    row_count = tokens.shape[0]
    gate_full, up_full = (
        lax.all_gather(ffn_gate, "fs", axis=0, tiled=True),
        lax.all_gather(ffn_up, "fs", axis=0, tiled=True),
    )
    down_full = lax.all_gather(ffn_down, "fs", axis=1, tiled=True)
    first_partial = channel_mix(tokens, gate_full, up_full, down_full)
    first = settle(first_partial, tokens, 0.5, norm_gain[0], norm_bias[0])
    key_cols = query_proj.shape[1]
    value_cols = value_proj.shape[1]
    query_full, key_full, value_full, outgate_full = (
        lax.all_gather(query_proj, "fs", axis=0, tiled=True),
        lax.all_gather(key_proj, "fs", axis=0, tiled=True),
        lax.all_gather(value_proj, "fs", axis=0, tiled=True),
        lax.all_gather(outgate_proj, "fs", axis=0, tiled=True),
    )
    joined_full = jnp.concatenate([query_full, key_full, value_full, outgate_full], axis=1)
    projected = jnp.dot(first, joined_full, preferred_element_type=jnp.float32)
    queries = projected[:, :key_cols] * DK ** (-0.5)
    keys_rows = projected[:, key_cols : 2 * key_cols]
    values = projected[:, 2 * key_cols : 2 * key_cols + value_cols]
    gates = projected[:, 2 * key_cols + value_cols :]
    head_count = key_cols // DK
    position = lax.axis_index("tp")
    key_start = position * (head_count * DK)
    value_start = position * (head_count * DV)
    rank_rows = jnp.dot(first, rank_down, preferred_element_type=jnp.float32)
    up_block = lax.dynamic_slice_in_dim(rank_up, key_start, head_count * DK, 1).astype(jnp.float32)
    bias_block = lax.dynamic_slice_in_dim(decay_bias, key_start, head_count * DK, 0)
    decay_source = jnp.dot(rank_rows, up_block, precision=FULL_ACCURACY) + bias_block
    decay_logarithm = jax.nn.log_sigmoid(decay_source) / GATE_SOFTNESS
    heads_out = gla_heads(
        queries.reshape(row_count, head_count, DK),
        keys_rows.reshape(row_count, head_count, DK),
        values.reshape(row_count, head_count, DV),
        decay_logarithm.reshape(row_count, head_count, DK),
    )
    scaled = heads_out * lax.rsqrt(jnp.mean(heads_out * heads_out, -1, keepdims=True) + HEAD_FLOOR)
    gain_block = lax.dynamic_slice_in_dim(head_gain, value_start, head_count * DV, 0)
    scaled = scaled * gain_block.reshape(head_count, DV)
    mixed = (scaled.reshape(row_count, head_count * DV) * jax.nn.silu(gates)).astype(jnp.bfloat16)
    mixer_partial = jnp.dot(
        mixed,
        lax.all_gather(output_proj, "fs", axis=1, tiled=True),
        preferred_element_type=jnp.float32,
    )
    second = settle(mixer_partial, first, 1.0, norm_gain[1], norm_bias[1])
    third_partial = channel_mix(second, gate_full, up_full, down_full)
    return settle(third_partial, second, 0.5, norm_gain[2], norm_bias[2])


def solution(mesh):
    return jax.shard_map(
        per_device,
        mesh=mesh,
        in_specs=(
            P(("rep", "fs"), None),
            P("fs", "tp"),
            P("fs", "tp"),
            P("tp", "fs"),
            P("fs", "tp"),
            P("fs", "tp"),
            P("fs", "tp"),
            P("fs", "tp"),
            P("tp", "fs"),
            P(),
            P(),
            P(),
            P(),
            P(),
            P(),
        ),
        out_specs=P(("rep", "fs"), None),
        check_vma=False,
    )
```

profile of v0, /device:TPU:0, one launch (start us, length us, event | category | flops | bytes accessed | tf_op | source)
XLA Modules:
  0.0 917.7 jit_solution(16187257873956331330)
XLA Ops:
  8.8 166.8 %all-gather.9.cloned.1.call-done = bf16[2048,2816]{1,0:T(8,128)(2,1)} async-done(((bf16[256,2816]{1,0:T(8,128)(2,1)}), bf16[2048,2816]{1,0:T(8,128)(2,1)}) %all-gather.9.cloned.1.call-update) | async-done | bytes 11534352 | tf_op jit(solution)/shard_map/all_gather | solution.py:98
  175.6 9.0 fusion.50
  184.6 154.7 %all-gather.11.cloned.1.call-done = bf16[2048,2816]{1,0:T(8,128)(2,1)} async-done(((bf16[256,2816]{1,0:T(8,128)(2,1)}), bf16[2048,2816]{1,0:T(8,128)(2,1)}) %all-gather.11.cloned.1.call-update) | async-done | bytes 11534352 | tf_op jit(solution)/shard_map/all_gather | solution.py:99
  339.3 163.6 %all-gather.13.cloned.1.call-done = bf16[2816,2048]{1,0:T(8,128)(2,1)} async-done(((bf16[2816,256]{1,0:T(8,128)(2,1)}), bf16[2816,2048]{1,0:T(8,128)(2,1)}) %all-gather.13.cloned.1.call-update) | async-done | bytes 11534352 | tf_op jit(solution)/shard_map/all_gather | solution.py:101
  502.9 15.5 %convolution_convert_fusion.2 = bf16[256,2048]{1,0:T(8,128)(2,1)} fusion(bf16[2816,2048]{1,0:T(8,128)(2,1)} %all-gather.13.cloned.1.call-done, bf16[256,2048]{1,0:T(8,128)(2,1)S(1)} %copy-done.2, bf16[2048,2816]{1,0:T(8,128)(2,1)} %all-gather.11.cloned.1.call-done, f32[256,2816]{1,0:T(8,128)} %fusion.50), kind=kOutput, calls=%fused_computation.45 | convolution fusion | flops 5910429696 | bytes 28049408 | tf_op jit(solution)/shard_map/dot_general | solution.py:76
  521.9 14.4 %all-reduce.6.cloned.1.call-start = ((), (), s32[]{:S(2)}) async-start(), calls=%async_computation.9 | async-start | bytes 2097152 | tf_op jit(solution)/shard_map/psum | solution.py:66
  539.7 40.0 %all-gather.15.cloned.1.call-done = bf16[2048,256]{1,0:T(8,128)(2,1)} async-done(((bf16[256,256]{1,0:T(8,128)(2,1)}), bf16[2048,256]{1,0:T(8,128)(2,1)}) %all-gather.15.cloned.1.call-update) | async-done | bytes 1048592 | tf_op jit(solution)/shard_map/all_gather | solution.py:107
  579.7 41.0 %all-gather.17.cloned.1.call-done = bf16[2048,256]{1,0:T(8,128)(2,1)} async-done(((bf16[256,256]{1,0:T(8,128)(2,1)}), bf16[2048,256]{1,0:T(8,128)(2,1)}) %all-gather.17.cloned.1.call-update) | async-done | bytes 1048592 | tf_op jit(solution)/shard_map/all_gather | solution.py:108
  620.7 50.0 %all-gather.19.cloned.1.call-done = bf16[2048,512]{1,0:T(8,128)(2,1)} async-done(((bf16[256,512]{1,0:T(8,128)(2,1)}), bf16[2048,512]{1,0:T(8,128)(2,1)}) %all-gather.19.cloned.1.call-update) | async-done | bytes 2097168 | tf_op jit(solution)/shard_map/all_gather | solution.py:109
  670.7 49.8 %all-gather.21.cloned.1.call-done = bf16[2048,512]{1,0:T(8,128)(2,1)} async-done(((bf16[256,512]{1,0:T(8,128)(2,1)}), bf16[2048,512]{1,0:T(8,128)(2,1)}) %all-gather.21.cloned.1.call-update) | async-done | bytes 2097168 | tf_op jit(solution)/shard_map/all_gather | solution.py:110
  720.4 3.9 fusion.20
  727.7 105.8 %while.13 = (s32[]{:T(128)}, f32[4,64,128]{2,1,0:T(8,128)S(1)}, f32[4,64,4,128]{3,1,2,0:T(8,128)}, f32[4,64,4,64]{3,2,1,0:T(4,128)S(1)}, f32[4,64,4,64]{3,2,1,0:...) while((s32[]{:T(128)}, f32[4,64,128]{2,1,0:T(8,128)S(1)}, ...), condition=%wide.region_5.6_spmd.clone, body=%wide.region_3.5_spmd.clone.sunk | while | flops 92475392 | bytes 10893944 | solution.py:57
  728.8 5.9 multiply_bitcast_fusion.2
  734.7 17.6 %fusion.91 = f32[4,64,1,64]{3,2,1,0:T(1,128)S(1)} fusion(f32[64,4,64,64]{2,1,3,0:T(4,128)S(1)} %multiply_bitcast_fusion.2, f32[64,4,64,1]{2,1,0,3:T(4,128)S(1)} %dynamic-slice_bitcast_fusion.4), kind=kOutput, calls=%fused_computation.1.clone.1 | convolution fusion | flops 12582912 | bytes 4325376 | tf_op jit(solution)/shard_map/while/body/eval_jaxpr/lshk,lhk,shk->hls/dot_general | solution.py:37
  755.2 5.9 multiply_bitcast_fusion.2
  761.1 17.6 %fusion.91 = f32[4,64,1,64]{3,2,1,0:T(1,128)S(1)} fusion(f32[64,4,64,64]{2,1,3,0:T(4,128)S(1)} %multiply_bitcast_fusion.2, f32[64,4,64,1]{2,1,0,3:T(4,128)S(1)} %dynamic-slice_bitcast_fusion.4), kind=kOutput, calls=%fused_computation.1.clone.1 | convolution fusion | flops 12582912 | bytes 4325376 | tf_op jit(solution)/shard_map/while/body/eval_jaxpr/lshk,lhk,shk->hls/dot_general | solution.py:37
  781.6 5.9 multiply_bitcast_fusion.2
  787.5 17.6 %fusion.91 = f32[4,64,1,64]{3,2,1,0:T(1,128)S(1)} fusion(f32[64,4,64,64]{2,1,3,0:T(4,128)S(1)} %multiply_bitcast_fusion.2, f32[64,4,64,1]{2,1,0,3:T(4,128)S(1)} %dynamic-slice_bitcast_fusion.4), kind=kOutput, calls=%fused_computation.1.clone.1 | convolution fusion | flops 12582912 | bytes 4325376 | tf_op jit(solution)/shard_map/while/body/eval_jaxpr/lshk,lhk,shk->hls/dot_general | solution.py:37
  808.0 5.9 multiply_bitcast_fusion.2
  813.9 17.6 %fusion.91 = f32[4,64,1,64]{3,2,1,0:T(1,128)S(1)} fusion(f32[64,4,64,64]{2,1,3,0:T(4,128)S(1)} %multiply_bitcast_fusion.2, f32[64,4,64,1]{2,1,0,3:T(4,128)S(1)} %dynamic-slice_bitcast_fusion.4), kind=kOutput, calls=%fused_computation.1.clone.1 | convolution fusion | flops 12582912 | bytes 4325376 | tf_op jit(solution)/shard_map/while/body/eval_jaxpr/lshk,lhk,shk->hls/dot_general | solution.py:37
  840.2 18.1 %all-reduce.6.cloned.1.call-done = bf16[256,2048]{1,0:T(8,128)(2,1)} async-done(((bf16[256,2048]{1,0:T(8,128)(2,1)}), bf16[256,2048]{1,0:T(8,128)(2,1)}) %all-reduce.6.cloned.1.call-update) | async-done | bytes 1048592 | tf_op jit(solution)/shard_map/psum | solution.py:66
  861.2 9.0 fusion.52
  870.3 15.5 %convolution_convert_fusion = bf16[256,2048]{1,0:T(8,128)(2,1)} fusion(bf16[2816,2048]{1,0:T(8,128)(2,1)} %all-gather.13.cloned.1.call-done, bf16[256,2048]{1,0:T(8,128)(2,1)S(1)} %add_convert_fusion.1, bf16[2048,2816]{1,0:T(8,128)(2,1)} %all-gather.11.cloned.1.call-done, f32[256,2816]{1,0:T(8,128)} %fusion.52), kind=kOutput, calls=%fused_computation.43 | convolution fusion | flops 5910429696 | bytes 28049408 | tf_op jit(solution)/shard_map/dot_general | solution.py:76
  885.9 20.8 %all-reduce.8.cloned.1.call-done = bf16[256,2048]{1,0:T(8,128)(2,1)} async-done(((bf16[256,2048]{1,0:T(8,128)(2,1)}), bf16[256,2048]{1,0:T(8,128)(2,1)}) %all-reduce.8.cloned.1.call-update) | async-done | bytes 1048592 | tf_op jit(solution)/shard_map/psum | solution.py:66
  (123 shorter events, 37.4 us)
Async XLA Ops:
  6.5 717.8 %copy-start = (bf16[2048,16]{0,1:T(8,128)(2,1)S(1)}, bf16[2048,16]{0,1:T(8,128)(2,1)}, u32[]{:S(2)}) copy-start(bf16[2048,16]{0,1:T(8,128)(2,1)} %param.26) | copy-start | bytes 196612
  6.5 169.1 %copy-start.2 = (bf16[256,2048]{1,0:T(8,128)(2,1)S(1)}, bf16[256,2048]{1,0:T(8,128)(2,1)}, u32[]{:S(2)}) copy-start(bf16[256,2048]{1,0:T(8,128)(2,1)} %param.17) | copy-start | bytes 3145732
  6.5 169.1 %all-gather.9.cloned.1.call-start = ((), (), s32[]{:S(2)}) async-start(), calls=%async_computation | async-start | bytes 12976128 | tf_op jit(solution)/shard_map/all_gather | solution.py:98
  7.3 332.0 %all-gather.11.cloned.1.call-start = ((), (), s32[]{:S(2)}) async-start(), calls=%async_computation.1 | async-start | bytes 12976128 | tf_op jit(solution)/shard_map/all_gather | solution.py:99
  8.0 494.9 %all-gather.13.cloned.1.call-start = ((), (), s32[]{:S(2)}) async-start(), calls=%async_computation.2 | async-start | bytes 12976128 | tf_op jit(solution)/shard_map/all_gather | solution.py:101
  8.7 527.8 %all-reduce.4.cloned.1.call-start = ((), (), s32[]{:S(2)}) async-start(), calls=%async_computation.3 | async-start | bytes 2097152 | tf_op jit(solution)/shard_map/psum | solution.py:66
  518.4 17.9 %copy-start.7 = (f32[3,2048]{1,0:T(4,128)S(1)}, f32[3,2048]{1,0:T(4,128)}, u32[]{:S(2)}) copy-start(f32[3,2048]{1,0:T(4,128)} %param.30) | copy-start | bytes 73732
  518.4 17.9 %copy-start.8 = (f32[3,2048]{1,0:T(4,128)S(1)}, f32[3,2048]{1,0:T(4,128)}, u32[]{:S(2)}) copy-start(f32[3,2048]{1,0:T(4,128)} %param.31) | copy-start | bytes 73732
  518.4 18.0 %copy-start.10 = (f32[512]{0:T(512)S(1)}, f32[512]{0:T(512)}, u32[]{:S(2)}) copy-start(f32[512]{0:T(512)} %param.28) | copy-start | bytes 6148
  518.4 18.0 %copy-start.9 = (f32[1024]{0:T(1024)S(1)}, f32[1024]{0:T(1024)}, u32[]{:S(2)}) copy-start(f32[1024]{0:T(1024)} %param.29) | copy-start | bytes 12292
  518.5 61.2 %all-gather.15.cloned.1.call-start = ((), (), s32[]{:S(2)}) async-start(), calls=%async_computation.4 | async-start | bytes 1179648 | tf_op jit(solution)/shard_map/all_gather | solution.py:107
  519.1 101.6 %all-gather.17.cloned.1.call-start = ((), (), s32[]{:S(2)}) async-start(), calls=%async_computation.5 | async-start | bytes 1179648 | tf_op jit(solution)/shard_map/all_gather | solution.py:108
  519.6 151.0 %all-gather.19.cloned.1.call-start = ((), (), s32[]{:S(2)}) async-start(), calls=%async_computation.6 | async-start | bytes 2359296 | tf_op jit(solution)/shard_map/all_gather | solution.py:109
  520.4 200.0 %all-gather.21.cloned.1.call-start = ((), (), s32[]{:S(2)}) async-start(), calls=%async_computation.7 | async-start | bytes 2359296 | tf_op jit(solution)/shard_map/all_gather | solution.py:110
  521.1 315.2 %all-gather.23.cloned.1.call-start = ((), (), s32[]{:S(2)}) async-start(), calls=%async_computation.8 | async-start | bytes 2359296 | tf_op jit(solution)/shard_map/all_gather | solution.py:139
  521.9 336.4 %all-reduce.6.cloned.1.call-start = ((), (), s32[]{:S(2)}) async-start(), calls=%async_computation.9 | async-start | bytes 2097152 | tf_op jit(solution)/shard_map/psum | solution.py:66
  536.6 1.8 copy-start.3
  724.3 1.2 copy-start.6
  724.3 1.2 copy-start.11
  726.0 1.5 slice-start
  840.2 66.5 %all-reduce.8.cloned.1.call-start = ((), (), s32[]{:S(2)}) async-start(), calls=%async_computation.10 | async-start | bytes 2097152 | tf_op jit(solution)/shard_map/psum | solution.py:66
  858.3 1.7 copy-start.4
  906.6 1.8 copy-start.5
  908.4 2.3 copy-start.1
Sparse Core Ops, SparseCore 0:
  9.5 166.0 all-gather.8
  177.8 161.4 all-gather.10
  341.4 161.4 all-gather.12
  518.6 17.5 all-reduce.3
  538.2 41.4 all-gather.14
  581.7 38.9 all-gather.16
  622.8 47.7 all-gather.18
  672.8 47.6 all-gather.20
  722.5 48.7 all-gather.22
  840.3 17.9 all-reduce.5
  886.0 20.5 all-reduce.7
where the time goes:
time: 924 us; the launch traced here: 918 us
  waiting for transfers between devices  710 us (77%)
  matrix products  135 us (15%)
  other arithmetic  39.5 us (4%)
  starting transfers between devices  14.8 us (2%)
  between operations  13.8 us (1%)
    all_gather x1, waiting for transfers between devices, per_device(): lax.all_gather(ffn_gate, 'fs', axis=0, tiled=True)  167 us
    all_gather x1, waiting for transfers between devices, per_device(): down_full = lax.all_gather(ffn_down, 'fs', axis=1, tiled=True)  164 us
    all_gather x1, waiting for transfers between devices, per_device(): lax.all_gather(ffn_up, 'fs', axis=0, tiled=True)  155 us
    dot_general x4, matrix products, advance(): jnp.einsum('lshk,lhk,shk->hls', weight, query_block, key_block, precision...  70.4 us
    all_gather x1, waiting for transfers between devices, per_device(): lax.all_gather(value_proj, 'fs', axis=0, tiled=True)  50 us
    all_gather x1, waiting for transfers between devices, per_device(): lax.all_gather(outgate_proj, 'fs', axis=0, tiled=True)  49.8 us
    all_gather x1, waiting for transfers between devices, per_device(): lax.all_gather(key_proj, 'fs', axis=0, tiled=True)  41 us
    all_gather x1, waiting for transfers between devices, per_device(): lax.all_gather(query_proj, 'fs', axis=0, tiled=True)  40 us
  transfers between devices with their start and end apart: 11, of which 9 were waited for; matrix products, arithmetic and copies ran while one was open for 14% of the time, Pallas kernels for 0%

commit v1 on v0

--- a/solution.py
+++ b/solution.py
@@ -98,7 +98,8 @@
         lax.all_gather(ffn_gate, "fs", axis=0, tiled=True),
         lax.all_gather(ffn_up, "fs", axis=0, tiled=True),
     )
-    down_full = lax.all_gather(ffn_down, "fs", axis=1, tiled=True)
+    pieces = lax.all_gather(ffn_down, "fs")
+    down_full = jnp.concatenate(pieces, axis=1)
     first_partial = channel_mix(tokens, gate_full, up_full, down_full)
     first = settle(first_partial, tokens, 0.5, norm_gain[0], norm_bias[0])
     key_cols = query_proj.shape[1]

time: 924 us -> 929 us (level)
  local copies, waits for them, and re-layouts: 4.66 us -> 24.7 us
  waiting for transfers between devices: 710 us -> 695 us
    all_gather x1, waiting for transfers between devices: 167 us -> 148 us  [per_device(): lax.all_gather(ffn_gate, 'fs', axis=0, tiled=True)]
    reshape x0 -> x1, local copies, waits for them, and re-layouts: none -> 15.5 us  [per_device(): down_full = jnp.concatenate(pieces, axis=1)]
  transfers between devices with their start and end apart: 11 -> 11, of which waited for: 9 -> 9; matrix products, arithmetic and copies ran while one was open for 14% -> 16% of each run, Pallas kernels for 0% -> 0%
where the time goes in v1:
time: 929 us; the launch traced here: 922 us
  waiting for transfers between devices  695 us (75%)
  matrix products  134 us (14%)
  other arithmetic  39.5 us (4%)
  local copies, waits for them, and re-layouts  24.7 us (3%)
  starting transfers between devices  14.8 us (2%)
  between operations  13.9 us (1%)
    all_gather x1, waiting for transfers between devices, per_device(): pieces = lax.all_gather(ffn_down, 'fs')  167 us
    all_gather x1, waiting for transfers between devices, per_device(): lax.all_gather(ffn_up, 'fs', axis=0, tiled=True)  155 us
    all_gather x1, waiting for transfers between devices, per_device(): lax.all_gather(ffn_gate, 'fs', axis=0, tiled=True)  148 us
    dot_general x4, matrix products, advance(): jnp.einsum('lshk,lhk,shk->hls', weight, query_block, key_block, precision...  70.4 us
    all_gather x1, waiting for transfers between devices, per_device(): lax.all_gather(value_proj, 'fs', axis=0, tiled=True)  50 us
    all_gather x1, waiting for transfers between devices, per_device(): lax.all_gather(outgate_proj, 'fs', axis=0, tiled=True)  49.8 us
    all_gather x1, waiting for transfers between devices, per_device(): lax.all_gather(key_proj, 'fs', axis=0, tiled=True)  41 us
    all_gather x1, waiting for transfers between devices, per_device(): lax.all_gather(query_proj, 'fs', axis=0, tiled=True)  40 us
  transfers between devices with their start and end apart: 11, of which 9 were waited for; matrix products, arithmetic and copies ran while one was open for 16% of the time, Pallas kernels for 0%

profile of v1, /device:TPU:0, one launch (start us, length us, event | category | flops | bytes accessed | tf_op | source)
XLA Modules:
  0.0 922.2 jit_solution(5175220783456150271)
XLA Ops:
  8.8 166.8 %all-gather.24.cloned.1.call-done = bf16[22528,256]{1,0:T(8,128)(2,1)} async-done(((bf16[2816,256]{1,0:T(8,128)(2,1)}), bf16[22528,256]{1,0:T(8,128)(2,1)}) %all-gather.24.cloned.1.call-update) | async-done | bytes 11534352 | tf_op jit(solution)/shard_map/all_gather | solution.py:101
  175.6 15.5 %copy.36 = bf16[2816,8,256]{0,2,1:T(8,128)(2,1)} copy(bf16[2816,8,256]{2,0,1:T(8,128)(2,1)} %bitcast.109) | data formatting | bytes 23068672 | tf_op jit(solution)/shard_map/reshape | solution.py:102
  191.1 148.2 %all-gather.10.cloned.1.call-done = bf16[2048,2816]{1,0:T(8,128)(2,1)} async-done(((bf16[256,2816]{1,0:T(8,128)(2,1)}), bf16[2048,2816]{1,0:T(8,128)(2,1)}) %all-gather.10.cloned.1.call-update) | async-done | bytes 11534352 | tf_op jit(solution)/shard_map/all_gather | solution.py:98
  339.3 9.0 fusion.50
  348.3 154.7 %all-gather.12.cloned.1.call-done = bf16[2048,2816]{1,0:T(8,128)(2,1)} async-done(((bf16[256,2816]{1,0:T(8,128)(2,1)}), bf16[2048,2816]{1,0:T(8,128)(2,1)}) %all-gather.12.cloned.1.call-update) | async-done | bytes 11534352 | tf_op jit(solution)/shard_map/all_gather | solution.py:99
  503.0 15.5 %convolution_convert_fusion.2 = bf16[256,2048]{1,0:T(8,128)(2,1)} fusion(bf16[2816,2048]{0,1:T(8,128)(2,1)} %bitcast.107, bf16[256,2048]{1,0:T(8,128)(2,1)S(1)} %copy-done.2, bf16[2048,2816]{1,0:T(8,128)(2,1)} %all-gather.12.cloned.1.call-done, f32[256,2816]{1,0:T(8,128)} %fusion.50), kind=kOutput, calls=%fused_computation.45 | convolution fusion | flops 5910429696 | bytes 28049408 | tf_op jit(solution)/shard_map/dot_general | solution.py:76
  522.0 14.4 %all-reduce.6.cloned.1.call-start = ((), (), s32[]{:S(2)}) async-start(), calls=%async_computation.8 | async-start | bytes 2097152 | tf_op jit(solution)/shard_map/psum | solution.py:66
  539.8 40.0 %all-gather.14.cloned.1.call-done = bf16[2048,256]{1,0:T(8,128)(2,1)} async-done(((bf16[256,256]{1,0:T(8,128)(2,1)}), bf16[2048,256]{1,0:T(8,128)(2,1)}) %all-gather.14.cloned.1.call-update) | async-done | bytes 1048592 | tf_op jit(solution)/shard_map/all_gather | solution.py:108
  579.8 41.0 %all-gather.16.cloned.1.call-done = bf16[2048,256]{1,0:T(8,128)(2,1)} async-done(((bf16[256,256]{1,0:T(8,128)(2,1)}), bf16[2048,256]{1,0:T(8,128)(2,1)}) %all-gather.16.cloned.1.call-update) | async-done | bytes 1048592 | tf_op jit(solution)/shard_map/all_gather | solution.py:109
  620.8 50.0 %all-gather.18.cloned.1.call-done = bf16[2048,512]{1,0:T(8,128)(2,1)} async-done(((bf16[256,512]{1,0:T(8,128)(2,1)}), bf16[2048,512]{1,0:T(8,128)(2,1)}) %all-gather.18.cloned.1.call-update) | async-done | bytes 2097168 | tf_op jit(solution)/shard_map/all_gather | solution.py:110
  670.8 49.8 %all-gather.20.cloned.1.call-done = bf16[2048,512]{1,0:T(8,128)(2,1)} async-done(((bf16[256,512]{1,0:T(8,128)(2,1)}), bf16[2048,512]{1,0:T(8,128)(2,1)}) %all-gather.20.cloned.1.call-update) | async-done | bytes 2097168 | tf_op jit(solution)/shard_map/all_gather | solution.py:111
  728.7 109.4 %while.13 = (s32[]{:T(128)}, f32[4,64,128]{2,1,0:T(8,128)S(1)}, f32[4,64,4,128]{3,1,2,0:T(8,128)}, f32[4,64,4,64]{3,2,1,0:T(4,128)S(1)}, f32[4,64,4,64]{3,2,1,0:...) while((s32[]{:T(128)}, f32[4,64,128]{2,1,0:T(8,128)S(1)}, ...), condition=%wide.region_5.6_spmd.clone, body=%wide.region_3.5_spmd.clone.sunk | while | flops 92475392 | bytes 10893944 | solution.py:57
  729.8 5.9 multiply_bitcast_fusion.2
  735.7 17.6 %fusion.91 = f32[4,64,1,64]{3,2,1,0:T(1,128)S(1)} fusion(f32[64,4,64,64]{2,1,3,0:T(4,128)S(1)} %multiply_bitcast_fusion.2, f32[64,4,64,1]{2,1,0,3:T(4,128)S(1)} %dynamic-slice_bitcast_fusion.4), kind=kOutput, calls=%fused_computation.1.clone.1 | convolution fusion | flops 12582912 | bytes 4325376 | tf_op jit(solution)/shard_map/while/body/eval_jaxpr/lshk,lhk,shk->hls/dot_general | solution.py:37
  757.1 5.9 multiply_bitcast_fusion.2
  763.0 17.6 %fusion.91 = f32[4,64,1,64]{3,2,1,0:T(1,128)S(1)} fusion(f32[64,4,64,64]{2,1,3,0:T(4,128)S(1)} %multiply_bitcast_fusion.2, f32[64,4,64,1]{2,1,0,3:T(4,128)S(1)} %dynamic-slice_bitcast_fusion.4), kind=kOutput, calls=%fused_computation.1.clone.1 | convolution fusion | flops 12582912 | bytes 4325376 | tf_op jit(solution)/shard_map/while/body/eval_jaxpr/lshk,lhk,shk->hls/dot_general | solution.py:37
  784.4 5.9 multiply_bitcast_fusion.2
  790.3 17.6 %fusion.91 = f32[4,64,1,64]{3,2,1,0:T(1,128)S(1)} fusion(f32[64,4,64,64]{2,1,3,0:T(4,128)S(1)} %multiply_bitcast_fusion.2, f32[64,4,64,1]{2,1,0,3:T(4,128)S(1)} %dynamic-slice_bitcast_fusion.4), kind=kOutput, calls=%fused_computation.1.clone.1 | convolution fusion | flops 12582912 | bytes 4325376 | tf_op jit(solution)/shard_map/while/body/eval_jaxpr/lshk,lhk,shk->hls/dot_general | solution.py:37
  811.7 5.9 multiply_bitcast_fusion.2
  817.6 17.6 %fusion.91 = f32[4,64,1,64]{3,2,1,0:T(1,128)S(1)} fusion(f32[64,4,64,64]{2,1,3,0:T(4,128)S(1)} %multiply_bitcast_fusion.2, f32[64,4,64,1]{2,1,0,3:T(4,128)S(1)} %dynamic-slice_bitcast_fusion.4), kind=kOutput, calls=%fused_computation.1.clone.1 | convolution fusion | flops 12582912 | bytes 4325376 | tf_op jit(solution)/shard_map/while/body/eval_jaxpr/lshk,lhk,shk->hls/dot_general | solution.py:37
  844.7 18.1 %all-reduce.6.cloned.1.call-done = bf16[256,2048]{1,0:T(8,128)(2,1)} async-done(((bf16[256,2048]{1,0:T(8,128)(2,1)}), bf16[256,2048]{1,0:T(8,128)(2,1)}) %all-reduce.6.cloned.1.call-update) | async-done | bytes 1048592 | tf_op jit(solution)/shard_map/psum | solution.py:66
  865.7 9.0 fusion.52
  874.8 15.5 %convolution_convert_fusion = bf16[256,2048]{1,0:T(8,128)(2,1)} fusion(bf16[2816,2048]{0,1:T(8,128)(2,1)} %bitcast.108, bf16[256,2048]{1,0:T(8,128)(2,1)S(1)} %add_convert_fusion.1, bf16[2048,2816]{1,0:T(8,128)(2,1)} %all-gather.12.cloned.1.call-done, f32[256,2816]{1,0:T(8,128)} %fusion.52), kind=kOutput, calls=%fused_computation.43 | convolution fusion | flops 5910429696 | bytes 28049408 | tf_op jit(solution)/shard_map/dot_general | solution.py:76
  890.4 20.8 %all-reduce.8.cloned.1.call-done = bf16[256,2048]{1,0:T(8,128)(2,1)} async-done(((bf16[256,2048]{1,0:T(8,128)(2,1)}), bf16[256,2048]{1,0:T(8,128)(2,1)}) %all-reduce.8.cloned.1.call-update) | async-done | bytes 1048592 | tf_op jit(solution)/shard_map/psum | solution.py:66
  (126 shorter events, 45.6 us)
Async XLA Ops:
  6.5 718.0 %copy-start = (bf16[2048,16]{0,1:T(8,128)(2,1)S(1)}, bf16[2048,16]{0,1:T(8,128)(2,1)}, u32[]{:S(2)}) copy-start(bf16[2048,16]{0,1:T(8,128)(2,1)} %param.26) | copy-start | bytes 196612
  6.5 169.1 %all-gather.24.cloned.1.call-start = ((), (), s32[]{:S(2)}) async-start(), calls=%async_computation.10 | async-start | bytes 12976128 | tf_op jit(solution)/shard_map/all_gather | solution.py:101
  7.3 332.0 %all-gather.10.cloned.1.call-start = ((), (), s32[]{:S(2)}) async-start(), calls=%async_computation | async-start | bytes 12976128 | tf_op jit(solution)/shard_map/all_gather | solution.py:98
  8.0 495.0 %all-gather.12.cloned.1.call-start = ((), (), s32[]{:S(2)}) async-start(), calls=%async_computation.1 | async-start | bytes 12976128 | tf_op jit(solution)/shard_map/all_gather | solution.py:99
  8.7 527.9 %all-reduce.4.cloned.1.call-start = ((), (), s32[]{:S(2)}) async-start(), calls=%async_computation.2 | async-start | bytes 2097152 | tf_op jit(solution)/shard_map/psum | solution.py:66
  175.6 163.7 %copy-start.2 = (bf16[256,2048]{1,0:T(8,128)(2,1)S(1)}, bf16[256,2048]{1,0:T(8,128)(2,1)}, u32[]{:S(2)}) copy-start(bf16[256,2048]{1,0:T(8,128)(2,1)} %param.17) | copy-start | bytes 3145732
  518.6 17.9 %copy-start.8 = (f32[3,2048]{1,0:T(4,128)S(1)}, f32[3,2048]{1,0:T(4,128)}, u32[]{:S(2)}) copy-start(f32[3,2048]{1,0:T(4,128)} %param.30) | copy-start | bytes 73732
  518.6 17.9 %copy-start.9 = (f32[3,2048]{1,0:T(4,128)S(1)}, f32[3,2048]{1,0:T(4,128)}, u32[]{:S(2)}) copy-start(f32[3,2048]{1,0:T(4,128)} %param.31) | copy-start | bytes 73732
  518.6 18.0 %copy-start.11 = (f32[512]{0:T(512)S(1)}, f32[512]{0:T(512)}, u32[]{:S(2)}) copy-start(f32[512]{0:T(512)} %param.28) | copy-start | bytes 6148
  518.6 18.0 %copy-start.10 = (f32[1024]{0:T(1024)S(1)}, f32[1024]{0:T(1024)}, u32[]{:S(2)}) copy-start(f32[1024]{0:T(1024)} %param.29) | copy-start | bytes 12292
  518.6 61.2 %all-gather.14.cloned.1.call-start = ((), (), s32[]{:S(2)}) async-start(), calls=%async_computation.3 | async-start | bytes 1179648 | tf_op jit(solution)/shard_map/all_gather | solution.py:108
  519.2 101.7 %all-gather.16.cloned.1.call-start = ((), (), s32[]{:S(2)}) async-start(), calls=%async_computation.4 | async-start | bytes 1179648 | tf_op jit(solution)/shard_map/all_gather | solution.py:109
  519.8 151.0 %all-gather.18.cloned.1.call-start = ((), (), s32[]{:S(2)}) async-start(), calls=%async_computation.5 | async-start | bytes 2359296 | tf_op jit(solution)/shard_map/all_gather | solution.py:110
  520.5 200.1 %all-gather.20.cloned.1.call-start = ((), (), s32[]{:S(2)}) async-start(), calls=%async_computation.6 | async-start | bytes 2359296 | tf_op jit(solution)/shard_map/all_gather | solution.py:111
  521.3 319.7 %all-gather.22.cloned.1.call-start = ((), (), s32[]{:S(2)}) async-start(), calls=%async_computation.7 | async-start | bytes 2359296 | tf_op jit(solution)/shard_map/all_gather | solution.py:140
  522.0 340.8 %all-reduce.6.cloned.1.call-start = ((), (), s32[]{:S(2)}) async-start(), calls=%async_computation.8 | async-start | bytes 2097152 | tf_op jit(solution)/shard_map/psum | solution.py:66
  536.7 1.8 copy-start.3
  724.5 1.2 copy-start.6
  726.1 1.6 slice-start
  838.0 3.3 copy-start.7
  844.7 66.5 %all-reduce.8.cloned.1.call-start = ((), (), s32[]{:S(2)}) async-start(), calls=%async_computation.9 | async-start | bytes 2097152 | tf_op jit(solution)/shard_map/psum | solution.py:66
  862.8 1.7 copy-start.4
  911.1 1.8 copy-start.5
  912.9 2.3 copy-start.1
  (1 other events, 1.2 us)
Sparse Core Ops, SparseCore 0:
  9.5 166.0 all-gather.23
  177.8 161.4 all-gather.9
  341.5 161.4 all-gather.11
  518.7 17.6 all-reduce.3
  538.3 41.4 all-gather.13
  581.8 38.9 all-gather.15
  623.0 47.7 all-gather.17
  672.9 47.6 all-gather.19
  722.6 48.8 all-gather.21
  844.8 17.9 all-reduce.5
  890.5 20.5 all-reduce.7
